TPU v7x, 32 devices: a whole 2x2x4 slice. The times are simulated.
32 devices in a mesh: sp: 16 (over z, y, x), tp: 2 (over core).
Axes of the slice: x: 2, y: 2, z: 4, core: 2. Of those that a mesh axis runs over, the one named last changes fastest.
Arguments:
- residual: bfloat16 [3072, 2048], P(('sp', 'tp')), may hold values from -6 to 6
- queries_narrow: bfloat16 [3072, 512], P('sp', 'tp'), may hold values from -24 to 24
- keys_narrow: bfloat16 [3072, 512], P('sp', 'tp'), may hold values from -24 to 24
- values_narrow: bfloat16 [3072, 512], P('sp', 'tp'), may hold values from -6 to 6
- queries_broad: bfloat16 [3072, 512], P('sp', 'tp'), may hold values from -24 to 24
- keys_broad: bfloat16 [3072, 512], P('sp', 'tp'), may hold values from -24 to 24
- values_broad: bfloat16 [3072, 512], P('sp', 'tp'), may hold values from -6 to 6
- gates_narrow: float32 [3072, 16], P('sp', 'tp'), may hold values from -3072 to 0, as said below
- gates_broad: float32 [3072, 8], P('sp', 'tp'), may hold values from -3072 to 0, as said below
- project_narrow: bfloat16 [512, 2048], P('tp'), may hold values from -0.5 to 0.5
- project_broad: bfloat16 [512, 2048], P('tp'), may hold values from -0.5 to 0.5
- norm_gain: float32 [2048], replicated, may hold values from 0.1 to 1.9
- up_weight: bfloat16 [2048, 8192], P('sp', 'tp'), may hold values from -0.125 to 0.125
- down_weight: bfloat16 [8192, 2048], P('tp', 'sp'), may hold values from -0.0625 to 0.0625
Outputs:
- layer_out: bfloat16 [3072, 2048], P(('sp', 'tp'))
Inputs may be any that keep to these rules, and one draw needn't show every extreme that they name: `gates_narrow`: each head's cumulative log gate never rises from one position to the next. `gates_broad`: each head's cumulative log gate never rises from one position to the next.
All inputs are finite; a program needn't handle non-finite values.
Results may differ from a plain program's by a relative error of at most 0.018.
Values may be sent and summed in bfloat16 or wider, within the bound.
A program may use at most 128 MiB of HBM per device.

v0:
```python
import functools

import jax
import jax.numpy as jnp
from jax import lax
from jax.experimental import pallas as pl
from jax.experimental.pallas import tpu as pltpu
from jax.sharding import PartitionSpec as P

A_DIM = 32
B_DIM = 64


def rms_scaled(mixed, norm_gain):
    mixed_wide = mixed.astype(jnp.float32)
    scale = lax.rsqrt(jnp.mean(mixed_wide * mixed_wide, axis=-1, keepdims=True) + 1e-06)
    return (mixed_wide * scale * norm_gain).astype(jnp.bfloat16)


def group_size(sp_count):
    return 8 if sp_count % 8 == 0 else sp_count


def head_columns(narrow_heads):
    ranges = [(h * A_DIM, (h + 1) * A_DIM, A_DIM) for h in range(narrow_heads)]
    return ranges + [(narrow_heads * A_DIM, narrow_heads * A_DIM + B_DIM, B_DIM)]


def attend_block(ranges, block, query, kv_all, gate_all):
    tokens, width = query.shape
    lane = lax.broadcasted_iota(jnp.int32, (tokens, width), 1)
    row = lax.broadcasted_iota(jnp.int32, (tokens, tokens), 0)
    column = lax.broadcasted_iota(jnp.int32, (tokens, tokens), 1)
    inside = [(lane >= low) & (lane < high) for low, high, _ in ranges]
    wide = query.astype(jnp.float32)
    head_queries = [jnp.where(mask, wide, 0.0).astype(jnp.bfloat16) for mask in inside]
    own_gates = gate_all[block]
    query_gates = [
        jnp.sum(jnp.where(row == column, own_gates[h : h + 1, :], 0.0), axis=1, keepdims=True)
        for h in range(len(ranges))
    ]

    def by_head(columns):
        spread = jnp.broadcast_to(columns[-1], (tokens, width))
        for mask, values in zip(inside[:-1], columns[:-1]):
            spread = jnp.where(mask, values, spread)
        return spread

    def step(key_block, state):
        peaks, totals, summed = state
        keys = kv_all[key_block, :, :width]
        values = kv_all[key_block, :, width:]
        key_gates = gate_all[key_block]
        allowed = column + (key_block - block) * tokens <= row
        new_peaks, new_totals, fades, terms = [], [], [], []
        for h, (_, _, size) in enumerate(ranges):
            scores = (
                lax.dot_general(
                    head_queries[h],
                    keys,
                    (((1,), (1,)), ((), ())),
                    preferred_element_type=jnp.float32,
                )
                * size ** (-0.5)
                + query_gates[h]
                - key_gates[h : h + 1, :]
            )
            scores = jnp.where(allowed, scores, -1e30)
            peak = jnp.maximum(peaks[h], jnp.max(scores, axis=1, keepdims=True))
            weights = jnp.exp(scores - peak)
            fade = jnp.exp(peaks[h] - peak)
            new_peaks.append(peak)
            new_totals.append(totals[h] * fade + jnp.sum(weights, axis=1, keepdims=True))
            fades.append(fade)
            terms.append(
                jnp.dot(
                    weights.astype(jnp.bfloat16), values, preferred_element_type=jnp.float32
                )
            )
        summed = summed * by_head(fades) + by_head(terms)
        return tuple(new_peaks), tuple(new_totals), summed

    heads = len(ranges)
    initial = (
        tuple(jnp.full((tokens, 1), -1e30, jnp.float32) for _ in range(heads)),
        tuple(jnp.zeros((tokens, 1), jnp.float32) for _ in range(heads)),
        jnp.zeros((tokens, width), jnp.float32),
    )
    _, totals, summed = lax.fori_loop(0, block + 1, step, initial)
    return (summed / by_head(totals)).astype(jnp.bfloat16)


def layer_kernel(
    count,
    group,
    ranges,
    q_ref,
    kv_ref,
    gate_ref,
    up_ref,
    down_ref,
    attended_out,
    up_out,
    down_out,
    q_all,
    kv_all,
    gate_all,
    attended,
    up_hold,
    down_hold,
    kv_sems,
    gate_sems,
    q_sems,
    back_sems,
    sems,
    own_sems,
):
    me = lax.axis_index("sp")
    head_groups = q_ref.shape[0]
    parts = count // head_groups
    my_heads = me % head_groups
    my_part = me // head_groups

    def block_of(part, slot):
        turn = slot % 2
        return slot * parts + (1 - turn) * part + turn * (parts - 1 - part)

    my_slot = me // parts
    my_turn = my_slot % 2
    place = me % parts
    reader_part = (1 - my_turn) * place + my_turn * (parts - 1 - place)
    up_rows = up_ref.shape[0]
    units = up_out.shape[1]
    columns = down_ref.shape[1]
    barrier = pltpu.get_barrier_semaphore()

    def hello(k, carry):
        pl.semaphore_signal(
            barrier,
            inc=1,
            device_id={"sp": (me + k) % count},
            device_id_type=pl.DeviceIdType.MESH,
        )
        return carry

    lax.fori_loop(1, count, hello, 0)
    pl.semaphore_wait(barrier, count - 1)

    def remote(source, target, sem_pair, first, second, peer):
        return pltpu.make_async_remote_copy(
            src_ref=source,
            dst_ref=target,
            send_sem=sem_pair.at[0, first],
            recv_sem=sem_pair.at[1, second],
            device_id={"sp": peer},
            device_id_type=pl.DeviceIdType.MESH,
        )

    def context_copies(k, owner):
        peer = (me + k) % count
        heads = peer % head_groups
        return (
            remote(kv_ref.at[heads], kv_all.at[owner], kv_sems, k, k, peer),
            remote(gate_ref.at[heads], gate_all.at[owner], gate_sems, k, k, peer),
        )

    def start_context(k, carry):
        for copy in context_copies(k, me):
            copy.start()
        return carry

    def wait_context(k, carry):
        for copy in context_copies(k, (me + count - k) % count):
            copy.wait_recv()
            copy.wait_send()
        return carry

    for heads in range(head_groups):
        reader = reader_part * head_groups + heads

        @pl.when(reader != me)
        def _():
            remote(q_ref.at[heads], q_all.at[my_slot], q_sems, heads, my_slot, reader).start()

        @pl.when(reader == me)
        def _():
            q_all[my_slot] = q_ref[heads]

    lax.fori_loop(1, count, start_context, 0)
    kv_all[me] = kv_ref[my_heads]
    gate_all[me] = gate_ref[my_heads]

    def up_source(chunk):
        return up_ref.at[:, pl.ds(pl.multiple_of(chunk * units, 128), units)]

    def down_source(chunk):
        return down_ref.at[pl.ds(pl.multiple_of(chunk * units, units), units), :]

    def up_target(owner):
        return up_out.at[pl.ds(pl.multiple_of(owner * up_rows, up_rows), up_rows), :]

    def down_target(owner):
        if len(down_out.shape) == 3:
            return down_out.at[owner]
        return down_out.at[:, pl.ds(pl.multiple_of(owner * columns, columns), columns)]

    def copies(k, target_owner):
        peer = (me + k) % count
        chunk = peer % group
        pairs = (
            (up_source(chunk), up_target(target_owner)),
            (down_source(chunk), down_target(target_owner)),
        )
        return [
            pltpu.make_async_remote_copy(
                src_ref=source,
                dst_ref=target,
                send_sem=sems.at[0, which, k],
                recv_sem=sems.at[1, which, k],
                device_id={"sp": peer},
                device_id_type=pl.DeviceIdType.MESH,
            )
            for which, (source, target) in enumerate(pairs)
        ]

    def start(k, carry):
        for copy in copies(k, me):
            copy.start()
        return carry

    def finish(k, carry):
        for copy in copies(k, (me + count - k) % count):
            copy.wait_recv()
            copy.wait_send()
        return carry

    lax.fori_loop(1, count, start, 0)
    own = me % group
    first = [
        pltpu.make_async_copy(up_source(own), up_hold, own_sems.at[0]),
        pltpu.make_async_copy(down_source(own), down_hold, own_sems.at[1]),
    ]
    for copy in first:
        copy.start()
    for copy in first:
        copy.wait()
    second = [
        pltpu.make_async_copy(up_hold, up_target(me), own_sems.at[0]),
        pltpu.make_async_copy(down_hold, down_target(me), own_sems.at[1]),
    ]
    for copy in second:
        copy.start()
    for heads in range(head_groups):
        reader = reader_part * head_groups + heads

        @pl.when(reader != me)
        def _():
            remote(q_ref.at[heads], q_all.at[my_slot], q_sems, heads, my_slot, reader).wait_send()

    for slot in range(head_groups):
        owner = block_of(my_part, slot)

        @pl.when(owner != me)
        def _():
            remote(q_ref.at[0], q_all.at[slot], q_sems, 0, slot, owner).wait_recv()

    lax.fori_loop(1, count, wait_context, 0)

    def attend(slot, carry):
        block = block_of(my_part, slot)
        attended[slot] = attend_block(ranges, block, q_all[slot], kv_all, gate_all)
        return carry

    lax.fori_loop(0, head_groups, attend, 0)
    for slot in range(head_groups):
        owner = block_of(my_part, slot)

        @pl.when(owner != me)
        def _():
            remote(
                attended.at[slot], attended_out.at[my_heads], back_sems, slot, my_heads, owner
            ).start()

        @pl.when(owner == me)
        def _():
            attended_out[my_heads] = attended[slot]

    for copy in second:
        copy.wait()
    lax.fori_loop(1, count, finish, 0)
    for slot in range(head_groups):
        owner = block_of(my_part, slot)

        @pl.when(owner != me)
        def _():
            remote(
                attended.at[slot], attended_out.at[my_heads], back_sems, slot, my_heads, owner
            ).wait_send()

    for heads in range(head_groups):
        reader = reader_part * head_groups + heads

        @pl.when(reader != me)
        def _():
            remote(
                attended.at[0], attended_out.at[heads], back_sems, 0, heads, reader
            ).wait_recv()


def attend_and_share(queries, keys_values, gates, ranges, up_weight, down_weight):
    head_groups, tokens, head_width = queries.shape
    count = lax.axis_size("sp")
    group = group_size(count)
    up_rows, unit_total = up_weight.shape
    columns = down_weight.shape[1]
    units = unit_total // group
    if columns % 128 == 0:
        down_shape = (units, count * columns)
    else:
        down_shape = (count, units, columns)
    attended, up_full, down_full = pl.pallas_call(
        functools.partial(layer_kernel, count, group, ranges),
        out_shape=(
            jax.ShapeDtypeStruct(queries.shape, queries.dtype),
            jax.ShapeDtypeStruct((count * up_rows, units), up_weight.dtype),
            jax.ShapeDtypeStruct(down_shape, down_weight.dtype),
        ),
        in_specs=[pl.BlockSpec(memory_space=pltpu.VMEM)] * 3
        + [pl.BlockSpec(memory_space=pl.ANY)] * 2,
        out_specs=[pl.BlockSpec(memory_space=pltpu.VMEM)]
        + [pl.BlockSpec(memory_space=pl.ANY)] * 2,
        scratch_shapes=[
            pltpu.VMEM(queries.shape, queries.dtype),
            pltpu.VMEM((count,) + keys_values.shape[1:], keys_values.dtype),
            pltpu.VMEM((count,) + gates.shape[1:], gates.dtype),
            pltpu.VMEM(queries.shape, queries.dtype),
            pltpu.VMEM((up_rows, units), up_weight.dtype),
            pltpu.VMEM((units, columns), down_weight.dtype),
            pltpu.SemaphoreType.DMA((2, count)),
            pltpu.SemaphoreType.DMA((2, count)),
            pltpu.SemaphoreType.DMA((2, head_groups)),
            pltpu.SemaphoreType.DMA((2, head_groups)),
            pltpu.SemaphoreType.DMA((2, 2, count)),
            pltpu.SemaphoreType.DMA((2,)),
        ],
        compiler_params=pltpu.CompilerParams(collective_id=0, has_side_effects=True),
        cost_estimate=pl.CostEstimate(
            flops=0, bytes_accessed=count * up_rows * units * 80, transcendentals=0
        ),
    )(queries, keys_values, gates, up_weight, down_weight)
    if columns % 128:
        down_full = down_full.transpose(1, 0, 2).reshape(units, count * columns)
    return attended, up_full, down_full


def gather_kernel(group, tp_count, rows_ref, out_ref, hold, sems, own_sems, pass_sems):
    sp = lax.axis_index("sp")
    tp = lax.axis_index("tp")
    base = (sp // group) * group
    me = sp - base
    barrier = pltpu.get_barrier_semaphore()
    for k in range(1, group):
        pl.semaphore_signal(
            barrier,
            inc=1,
            device_id={"sp": base + (me + k) % group},
            device_id_type=pl.DeviceIdType.MESH,
        )
    for j in range(1, tp_count):
        pl.semaphore_signal(
            barrier,
            inc=1,
            device_id={"tp": (tp + j) % tp_count},
            device_id_type=pl.DeviceIdType.MESH,
        )
    pl.semaphore_wait(barrier, group + tp_count - 2)

    def across(k, owner):
        return pltpu.make_async_remote_copy(
            src_ref=rows_ref,
            dst_ref=out_ref.at[tp, owner],
            send_sem=sems.at[0, k],
            recv_sem=sems.at[1, k],
            device_id={"sp": base + (me + k) % group},
            device_id_type=pl.DeviceIdType.MESH,
        )

    def beside(j, k, source, tp_owner, owner):
        return pltpu.make_async_remote_copy(
            src_ref=source,
            dst_ref=out_ref.at[tp_owner, owner],
            send_sem=pass_sems.at[0, j, k],
            recv_sem=pass_sems.at[1, j, k],
            device_id={"tp": (tp + j) % tp_count},
            device_id_type=pl.DeviceIdType.MESH,
        )

    for k in range(1, group):
        across(k, me).start()
    for j in range(1, tp_count):
        beside(j, 0, rows_ref, tp, me).start()
    own = pltpu.make_async_copy(rows_ref, hold, own_sems.at[0])
    own.start()
    own.wait()
    own = pltpu.make_async_copy(hold, out_ref.at[tp, me], own_sems.at[1])
    own.start()
    own.wait()
    for k in range(1, group):
        owner = (me + group - k) % group
        across(k, owner).wait_recv()
        for j in range(1, tp_count):
            beside(j, k, out_ref.at[tp, owner], tp, owner).start()
    for k in range(1, group):
        across(k, me).wait_send()
    for j in range(1, tp_count):
        for k in range(group):
            owner = (me + group - k) % group
            copy = beside(j, k, rows_ref, (tp + tp_count - j) % tp_count, owner)
            copy.wait_send()
            copy.wait_recv()


def gather_rows(rows):
    group = group_size(lax.axis_size("sp"))
    tp_count = lax.axis_size("tp")
    return pl.pallas_call(
        functools.partial(gather_kernel, group, tp_count),
        out_shape=jax.ShapeDtypeStruct((tp_count, group) + rows.shape, rows.dtype),
        in_specs=[pl.BlockSpec(memory_space=pl.ANY)],
        out_specs=pl.BlockSpec(memory_space=pl.ANY),
        scratch_shapes=[
            pltpu.VMEM(rows.shape, rows.dtype),
            pltpu.SemaphoreType.DMA((2, group)),
            pltpu.SemaphoreType.DMA((2,)),
            pltpu.SemaphoreType.DMA((2, tp_count, group)),
        ],
        compiler_params=pltpu.CompilerParams(collective_id=1, has_side_effects=True),
    )(rows)


def return_kernel(group, parts_ref, out_ref, hold, sems, own_sems):
    sp = lax.axis_index("sp")
    base = (sp // group) * group
    me = sp - base
    barrier = pltpu.get_barrier_semaphore()
    for k in range(1, group):
        pl.semaphore_signal(
            barrier,
            inc=1,
            device_id={"sp": base + (me + k) % group},
            device_id_type=pl.DeviceIdType.MESH,
        )
    pl.semaphore_wait(barrier, group - 1)

    def across(k, owner):
        peer = (me + k) % group
        return pltpu.make_async_remote_copy(
            src_ref=parts_ref.at[peer],
            dst_ref=out_ref.at[owner],
            send_sem=sems.at[0, k],
            recv_sem=sems.at[1, k],
            device_id={"sp": base + peer},
            device_id_type=pl.DeviceIdType.MESH,
        )

    for k in range(1, group):
        across(k, me).start()
    own = pltpu.make_async_copy(parts_ref.at[me], hold, own_sems.at[0])
    own.start()
    own.wait()
    own = pltpu.make_async_copy(hold, out_ref.at[me], own_sems.at[1])
    own.start()
    own.wait()
    for k in range(1, group):
        copy = across(k, (me + group - k) % group)
        copy.wait_recv()
        copy.wait_send()


def return_parts(parts):
    group = parts.shape[0]
    return pl.pallas_call(
        functools.partial(return_kernel, group),
        out_shape=jax.ShapeDtypeStruct(parts.shape, parts.dtype),
        in_specs=[pl.BlockSpec(memory_space=pl.ANY)],
        out_specs=pl.BlockSpec(memory_space=pl.ANY),
        scratch_shapes=[
            pltpu.VMEM(parts.shape[1:], parts.dtype),
            pltpu.SemaphoreType.DMA((2, group)),
            pltpu.SemaphoreType.DMA((2,)),
        ],
        compiler_params=pltpu.CompilerParams(collective_id=2, has_side_effects=True),
    )(parts)


def local(
    residual,
    queries_narrow,
    keys_narrow,
    values_narrow,
    queries_broad,
    keys_broad,
    values_broad,
    gates_narrow,
    gates_broad,
    project_narrow,
    project_broad,
    norm_gain,
    up_weight,
    down_weight,
):
    tokens = queries_narrow.shape[0]
    head_groups = gates_broad.shape[1]
    narrow_heads = gates_narrow.shape[1] // head_groups
    ranges = head_columns(narrow_heads)

    def by_group(narrow, broad):
        return jnp.concatenate(
            [part.reshape(tokens, head_groups, -1) for part in (narrow, broad)], axis=-1
        ).transpose(1, 0, 2)

    gates = jnp.concatenate(
        [gates_narrow.reshape(tokens, head_groups, narrow_heads), gates_broad[..., None]], axis=-1
    ).transpose(1, 2, 0)
    gates = jnp.pad(gates, ((0, 0), (0, -gates.shape[1] % 8), (0, 0)))
    attended, up_full, down_full = attend_and_share(
        by_group(queries_narrow, queries_broad),
        jnp.concatenate(
            [by_group(keys_narrow, keys_broad), by_group(values_narrow, values_broad)], axis=-1
        ),
        gates,
        ranges,
        up_weight,
        down_weight,
    )
    rows_first = attended.transpose(1, 0, 2)
    split = narrow_heads * A_DIM
    attended_narrow = rows_first[..., :split].reshape(tokens, -1)
    attended_broad = rows_first[..., split:].reshape(tokens, -1)
    projected = lax.psum_scatter(
        (
            jnp.dot(attended_narrow, project_narrow, preferred_element_type=jnp.float32)
            + jnp.dot(attended_broad, project_broad, preferred_element_type=jnp.float32)
        ).astype(jnp.bfloat16),
        "tp",
        scatter_dimension=0,
        tiled=True,
    ).astype(jnp.float32)
    mixed = (residual.astype(jnp.float32) + projected).astype(jnp.bfloat16)
    features = gather_rows(rms_scaled(mixed, norm_gain))
    tp_count, group, rows, width = features.shape
    up_total = jnp.dot(
        features.reshape(tp_count * group * rows, width),
        up_full,
        preferred_element_type=jnp.float32,
    )
    hidden = jnp.square(jax.nn.relu(up_total)).astype(jnp.bfloat16)
    down_term = jnp.dot(hidden, down_full, preferred_element_type=jnp.float32)
    parts = lax.psum_scatter(
        down_term.astype(jnp.bfloat16).reshape(features.shape),
        "tp",
        scatter_dimension=0,
        tiled=False,
    )
    summed_rows = jnp.sum(return_parts(parts).astype(jnp.float32), axis=0)
    return (mixed.astype(jnp.float32) + summed_rows).astype(jnp.bfloat16)


def solution(mesh):
    return jax.shard_map(
        local,
        mesh=mesh,
        in_specs=(
            P(("sp", "tp"), None),
            P("sp", "tp"),
            P("sp", "tp"),
            P("sp", "tp"),
            P("sp", "tp"),
            P("sp", "tp"),
            P("sp", "tp"),
            P("sp", "tp"),
            P("sp", "tp"),
            P("tp", None),
            P("tp", None),
            P(),
            P("sp", "tp"),
            P("tp", "sp"),
        ),
        out_specs=P(("sp", "tp"), None),
        check_vma=False,
    )
```

profile of v0, /device:TPU:0, one launch (start us, length us, event | category | flops | bytes accessed | tf_op | source)
XLA Modules:
  0.0 327.7 jit_solution(5625753208808115502)
XLA Ops:
  6.5 0.8 broadcast_in_dim.2
  7.3 0.7 reshape.48
  8.0 1.0 copy.15
  9.2 1.0 copy.19
  10.4 1.0 copy.23
  11.5 1.0 copy.16
  12.7 1.0 copy.20
  13.9 1.0 copy.24
  15.1 0.6 pad.4.gate_ref
  15.7 0.8 maximum_bitcast_fusion.q_ref
  16.7 0.8 pad_maximum_fusion.kv_ref
  17.5 125.1 %shard_map.136 = (bf16[4,192,128]{2,1,0:T(8,128)(2,1)}, bf16[2048,512]{1,0:T(8,128)(2,1)}, bf16[512,2048]{1,0:T(8,128)(2,1)}) custom-call(bf16[4,192,128]{2,1,0:T(8,128)(2,1)} %maximum_bitcast_fusion.q_ref, bf16[4,192,256]{2,1,0:T(8,128)(2,1)} %pad_maximum_fusion.kv_ref, f32[4,8,192]{2,1,0:T(8,128)} %pad.4.gate_ref, bf16[128,4096]{1,0:T(8,128)(2,1)} %up_ref.1, ...), custom_call_target="tpu_custom_call" | custom-call | bytes 83886080 | tf_op jit(solution)/shard_map/pallas_call | solution.py:321
  142.6 1.1 fusion.8
  144.0 0.4 fusion.9
  144.4 1.3 fusion.2
  145.9 38.0 %reduce-scatter.3.cloned.1.call-done = bf16[96,2048]{1,0:T(8,128)(2,1)} async-done(((bf16[192,2048]{1,0:T(8,128)(2,1)}), bf16[96,2048]{1,0:T(8,128)(2,1)}) %reduce-scatter.3.cloned.1.call-update) | async-done | bytes 393232 | tf_op jit(solution)/shard_map/reduce_scatter | solution.py:540
  183.9 1.2 fusion.3
  185.1 1.9 fusion.5.rows_ref
  187.0 50.4 %shard_map.137 = bf16[2,8,96,2048]{3,2,1,0:T(8,128)(2,1)} custom-call(bf16[96,2048]{1,0:T(8,128)(2,1)} %fusion.5.rows_ref), custom_call_target="tpu_custom_call" | custom-call | tf_op jit(solution)/shard_map/pallas_call | solution.py:426
  237.5 11.1 %convolution_convert_fusion = bf16[1536,2048]{1,0:T(8,128)(2,1)} fusion(bf16[512,2048]{1,0:T(8,128)(2,1)} %get-tuple-element.10, bf16[1536,2048]{1,0:T(8,128)(2,1)} %bitcast.32, bf16[2048,512]{1,0:T(8,128)(2,1)S(1)} %copy-done.5), kind=kOutput, calls=%fused_computation | convolution fusion | flops 6447955968 | bytes 16777216 | tf_op jit(solution)/shard_map/dot_general | solution.py:558
  248.6 19.8 %reduce-scatter.5.cloned.1.call-done = bf16[1,8,96,2048]{3,2,1,0:T(8,128)(2,1)} async-done(((bf16[2,8,96,2048]{3,2,1,0:T(8,128)(2,1)}), bf16[1,8,96,2048]{3,2,1,0:T(8,128)(2,1)}) %reduce-scatter.5.cloned.1.call-update) | async-done | bytes 3145744 | tf_op jit(solution)/shard_map/reduce_scatter | solution.py:559
  268.3 49.0 %shard_map.138 = bf16[8,96,2048]{2,1,0:T(8,128)(2,1)} custom-call(bf16[8,96,2048]{2,1,0:T(8,128)(2,1)} %bitcast.33), custom_call_target="tpu_custom_call" | custom-call | tf_op jit(solution)/shard_map/pallas_call | solution.py:482
  317.4 2.6 convert_reduce_fusion
  320.0 0.9 fusion.6
  (27 shorter events, 1.6 us)
Async XLA Ops:
  6.5 137.5 %copy-start = (bf16[256,2048]{1,0:T(8,128)(2,1)S(1)}, bf16[256,2048]{1,0:T(8,128)(2,1)}, u32[]{:S(2)}) copy-start(bf16[256,2048]{1,0:T(8,128)(2,1)} %param.23) | copy-start | bytes 3145732
  6.5 177.3 %reduce-scatter.3.cloned.1.call-start = ((), (), s32[]{:S(2)}) async-start(), calls=%async_computation.2 | async-start | bytes 1179648 | tf_op jit(solution)/shard_map/reduce_scatter | solution.py:540
  17.5 127.0 %copy-start.3 = (bf16[256,2048]{1,0:T(8,128)(2,1)S(1)}, bf16[256,2048]{1,0:T(8,128)(2,1)}, u32[]{:S(2)}) copy-start(bf16[256,2048]{1,0:T(8,128)(2,1)} %param.24) | copy-start | bytes 3145732
  144.0 39.9 %copy-start.1 = (bf16[96,2048]{1,0:T(8,128)(2,1)S(1)}, bf16[96,2048]{1,0:T(8,128)(2,1)}, u32[]{:S(2)}) copy-start(bf16[96,2048]{1,0:T(8,128)(2,1)} %param.14) | copy-start | bytes 1179652
  144.4 40.7 %copy-start.4 = (f32[2048]{0:T(1024)S(1)}, f32[2048]{0:T(1024)}, u32[]{:S(2)}) copy-start(f32[2048]{0:T(1024)} %param.25) | copy-start | bytes 24580
  145.8 122.5 %reduce-scatter.5.cloned.1.call-start = ((), (), s32[]{:S(2)}) async-start(), calls=%async_computation.3 | async-start | bytes 9437184 | tf_op jit(solution)/shard_map/reduce_scatter | solution.py:559
  187.0 50.5 %copy-start.5 = (bf16[2048,512]{1,0:T(8,128)(2,1)S(1)}, bf16[2048,512]{1,0:T(8,128)(2,1)}, u32[]{:S(2)}) copy-start(bf16[2048,512]{1,0:T(8,128)(2,1)} %get-tuple-element.9) | copy-start | bytes 6291460
  317.3 2.6 copy-start.2
Sparse Core Ops, SparseCore 0:
  145.9 37.8 reduce-scatter.2
  248.7 19.6 reduce-scatter.4
where the time goes:
time: 328 us
  Pallas kernels  225 us (69%)
  waiting for transfers between devices  57.8 us (18%)
  between operations  13.6 us (4%)
  matrix products  12.8 us (4%)
  local copies, waits for them, and re-layouts  10.5 us (3%)
  other arithmetic  8.42 us (3%)
    pallas_call x1, Pallas kernels, attend_and_share(): pl.pallas_call(functools.partial(layer_kernel, count, group, ranges), out...  125 us
    pallas_call x1, Pallas kernels, gather_rows(): pl.pallas_call(functools.partial(gather_kernel, group, tp_count), out_sha...  50.4 us
    pallas_call x1, Pallas kernels, return_parts(): pl.pallas_call(functools.partial(return_kernel, group), out_shape=jax.Sha...  49 us
    reduce_scatter x1, waiting for transfers between devices, local(): lax.psum_scatter((jnp.dot(attended_narrow, project_narrow, preferred_elem...  38 us
    reduce_scatter x1, waiting for transfers between devices, local(): lax.psum_scatter(down_term.astype(jnp.bfloat16).reshape(features.shape),...  19.8 us
    dot_general x1, matrix products, local(): down_term = jnp.dot(hidden, down_full, preferred_element_type=jnp.float32)  11.1 us
  transfers between devices with their start and end apart: 2, of which 2 were waited for; matrix products, arithmetic and copies ran while one was open for 0% of the time, Pallas kernels for 0%

commit v1 on v0

--- a/solution.py
+++ b/solution.py
@@ -566,9 +566,781 @@
     return (mixed.astype(jnp.float32) + summed_rows).astype(jnp.bfloat16)
 
 
+LOG2E = 1.4426950408889634
+PIECES = 3
+GATE_ROWS = 16
+
+
+def split_pieces(values):
+    pieces = []
+    rest = values
+    for _ in range(PIECES):
+        piece = rest.astype(jnp.bfloat16).astype(jnp.float32)
+        pieces.append(piece)
+        rest = rest - piece
+    return pieces
+
+
+def pad_rows(values, rows):
+    return jnp.concatenate(
+        [values, jnp.zeros((rows - values.shape[0], values.shape[1]), values.dtype)], axis=0
+    )
+
+
+def pad_lanes(values, lanes):
+    return jnp.concatenate(
+        [values, jnp.zeros((values.shape[0], lanes - values.shape[1]), values.dtype)], axis=1
+    )
+
+
+def fused_kernel(
+    count,
+    group,
+    head_groups,
+    ranges,
+    residual_ref,
+    qn_ref,
+    kn_ref,
+    vn_ref,
+    qb_ref,
+    kb_ref,
+    vb_ref,
+    gn_ref,
+    gb_ref,
+    gain_ref,
+    pn_ref,
+    pb_ref,
+    up_ref,
+    down_ref,
+    out_ref,
+    q_send,
+    kv_send,
+    gate_send,
+    q_all,
+    kv_all,
+    gate_all,
+    key_gates,
+    v_turned,
+    q_wide,
+    acc,
+    attended,
+    attended_in,
+    project,
+    mixed,
+    normed,
+    up_all,
+    down_all,
+    features,
+    hidden,
+    part_out,
+    part_in,
+    return_out,
+    return_in,
+    kv_line,
+    gate_line,
+    kv_plane,
+    gate_plane,
+    q_sems,
+    back_sems,
+    project_own,
+    project_sems,
+    weight_sems,
+    own_sems,
+    across_sems,
+    beside_sems,
+    part_sems,
+    return_sems,
+):
+    me = lax.axis_index("sp")
+    tp = lax.axis_index("tp")
+    other = 1 - tp
+    planes = head_groups
+    parts = count // planes
+    plane = me // parts
+    lane = me % parts
+    base = (me // group) * group
+    local = me - base
+    tokens, _ = qn_ref.shape
+    rows, width = residual_ref.shape
+    heads = len(ranges)
+    head_width = q_send.shape[2]
+    narrow_width = ranges[-1][0]
+    broad_width = head_width - narrow_width
+    span = 2 * tokens
+    barrier = pltpu.get_barrier_semaphore()
+
+    def remote(source, target, send, recv, sp, core):
+        return pltpu.make_async_remote_copy(
+            src_ref=source,
+            dst_ref=target,
+            send_sem=send,
+            recv_sem=recv,
+            device_id={"sp": sp, "tp": core},
+            device_id_type=pl.DeviceIdType.MESH,
+        )
+
+    def hello(k, carry):
+        flat = (me * 2 + tp + k) % (count * 2)
+        pl.semaphore_signal(
+            barrier,
+            inc=1,
+            device_id={"sp": flat // 2, "tp": flat % 2},
+            device_id_type=pl.DeviceIdType.MESH,
+        )
+        return carry
+
+    lax.fori_loop(1, count * 2, hello, 0)
+
+    def by_group(narrow_ref, broad_ref, h):
+        return [
+            narrow_ref[:, h * narrow_width : (h + 1) * narrow_width],
+            broad_ref[:, h * broad_width : (h + 1) * broad_width],
+        ]
+
+    narrow_heads = heads - 1
+    gates = pad_lanes(jnp.concatenate([gn_ref[...], gb_ref[...]], axis=1), 128)
+    gates = pad_rows(gates, -(-tokens // 128) * 128).T[:, :tokens]
+    for h in range(head_groups):
+        kv_send[h] = jnp.concatenate(
+            by_group(kn_ref, kb_ref, h) + by_group(vn_ref, vb_ref, h), axis=1
+        )
+        q_send[h] = jnp.concatenate(by_group(qn_ref, qb_ref, h), axis=1)
+        lines = []
+        for i, (_, _, size) in enumerate(ranges):
+            if i < narrow_heads:
+                source = h * narrow_heads + i
+            else:
+                source = head_groups * narrow_heads + h
+            lines += split_pieces(gates[source : source + 1] * size**0.5)
+        lines += [jnp.ones((PIECES, tokens), jnp.float32)]
+        gate_send[h] = pad_rows(jnp.concatenate(lines, axis=0), GATE_ROWS).astype(jnp.bfloat16)
+
+    pl.semaphore_wait(barrier, count * 2 - 1)
+
+    def line_copies(j, owner):
+        target = (plane + j) % planes
+        peer = target * parts + lane
+        return (
+            remote(
+                kv_send.at[target], kv_all.at[owner], kv_line.at[0, j], kv_line.at[1, j], peer, tp
+            ),
+            remote(
+                gate_send.at[target],
+                gate_all.at[owner],
+                gate_line.at[0, j],
+                gate_line.at[1, j],
+                peer,
+                tp,
+            ),
+        )
+
+    def line_owner(j):
+        return ((plane + planes - j) % planes) * parts + lane
+
+    def plane_copies(j, k, kv_source, gate_source, owner):
+        peer = plane * parts + (lane + k) % parts
+        return (
+            remote(
+                kv_source,
+                kv_all.at[owner],
+                kv_plane.at[0, j, k],
+                kv_plane.at[1, j, k],
+                peer,
+                tp,
+            ),
+            remote(
+                gate_source,
+                gate_all.at[owner],
+                gate_plane.at[0, j, k],
+                gate_plane.at[1, j, k],
+                peer,
+                tp,
+            ),
+        )
+
+    for j in range(1, planes):
+        for copy in line_copies(j, me):
+            copy.start()
+    for k in range(1, parts):
+        for copy in plane_copies(0, k, kv_send.at[plane], gate_send.at[plane], me):
+            copy.start()
+    kv_all[me] = kv_send[plane]
+    gate_all[me] = gate_send[plane]
+
+    double = me // 2
+    reader_part = jnp.where(double < parts, double, 2 * parts - 1 - double)
+    my_slot = 2 * (double // parts) + me % 2
+
+    def tile_double(tile):
+        return tile * (2 * parts - 1 - lane) + (1 - tile) * lane
+
+    for h in range(head_groups):
+        reader = h * parts + reader_part
+
+        @pl.when(reader != me)
+        def _():
+            remote(
+                q_send.at[h], q_all.at[my_slot], q_sems.at[0, h], q_sems.at[1, my_slot], reader, tp
+            ).start()
+
+        @pl.when(reader == me)
+        def _():
+            q_all[my_slot] = q_send[h]
+
+    def project_pairs(h):
+        pairs = []
+        for source, low, size in (
+            (pn_ref, 0, narrow_width),
+            (pb_ref, narrow_width, broad_width),
+        ):
+            pairs.append(
+                (
+                    source.at[h * size : (h + 1) * size, :],
+                    project.at[tp * head_groups + h, low : low + size, :],
+                )
+            )
+        return pairs
+
+    def project_copies(h):
+        own, away = [], []
+        for i, (source, target) in enumerate(project_pairs(h)):
+            own.append(pltpu.make_async_copy(source, target, project_own.at[h, i]))
+            away.append(
+                remote(
+                    source,
+                    target,
+                    project_sems.at[0, h, i],
+                    project_sems.at[1, h, i],
+                    me,
+                    other,
+                )
+            )
+        return own, away
+
+    for h in range(head_groups):
+        own, away = project_copies(h)
+        for copy in own + away:
+            copy.start()
+
+    units = up_all.shape[2]
+
+    def up_source(chunk):
+        return up_ref.at[:, pl.ds(pl.multiple_of(chunk * units, 128), units)]
+
+    def down_source(chunk):
+        return down_ref.at[pl.ds(pl.multiple_of(chunk * units, units), units), :]
+
+    def weight_copy(which, k, owner):
+        peer = (me + k) % count
+        chunk = peer % group
+        source = up_source(chunk) if which == 0 else down_source(chunk)
+        target = up_all.at[owner] if which == 0 else down_all.at[owner]
+        return remote(
+            source, target, weight_sems.at[0, which, k], weight_sems.at[1, which, k], peer, tp
+        )
+
+    own_weights = [
+        pltpu.make_async_copy(up_source(local), up_all.at[me], own_sems.at[0]),
+        pltpu.make_async_copy(down_source(local), down_all.at[me], own_sems.at[1]),
+    ]
+    for copy in own_weights:
+        copy.start()
+
+    for j in range(1, planes):
+        owner = line_owner(j)
+        for copy in line_copies(j, owner):
+            copy.wait_recv()
+        for k in range(1, parts):
+            for copy in plane_copies(j, k, kv_all.at[owner], gate_all.at[owner], owner):
+                copy.start()
+
+    def start_weights(which):
+        def start(k, carry):
+            weight_copy(which, k, me).start()
+            return carry
+
+        lax.fori_loop(1, count, start, 0)
+
+    start_weights(0)
+    start_weights(1)
+
+    for j in range(planes):
+        for k in range(1, parts):
+            owner = ((plane + planes - j) % planes) * parts + (lane + parts - k) % parts
+            for copy in plane_copies(j, k, kv_all.at[owner], gate_all.at[owner], owner):
+                copy.wait_recv()
+
+    def turn(pair, carry):
+        values = kv_all[pl.ds(2 * pair, 2), :, head_width:].reshape(span, head_width)
+        v_turned[pair] = values.astype(jnp.float32).T.astype(jnp.bfloat16)
+        for i in range(2):
+            block = pad_rows(gate_all[2 * pair + i].astype(jnp.float32), 128)
+            block = pad_lanes(block, -(-tokens // 128) * 128).T[:tokens]
+            key_gates[2 * pair + i] = block.astype(jnp.bfloat16)
+        return carry
+
+    lax.fori_loop(0, count // 2, turn, 0)
+
+    for slot in range(4):
+        owner = 2 * tile_double(slot // 2) + slot % 2
+
+        @pl.when(owner != me)
+        def _():
+            remote(
+                q_send.at[0], q_all.at[slot], q_sems.at[0, 0], q_sems.at[1, slot], owner, tp
+            ).wait_recv()
+
+    lane_id = lax.broadcasted_iota(jnp.int32, (span, head_width), 1)
+    first_one = heads * PIECES
+
+    def attend(tile, carry):
+        double_block = tile_double(tile)
+        query = q_all[pl.ds(2 * tile, 2)].reshape(span, head_width).astype(jnp.float32)
+        own_gates = (
+            key_gates[pl.ds(2 * double_block, 2)].reshape(span, head_width).astype(jnp.float32)
+        )
+        for i, (low, high, _) in enumerate(ranges):
+            left = jnp.where((lane_id >= low) & (lane_id < high), query, 0.0)
+            moved = pltpu.roll(own_gates, first_one - i * PIECES, 1)
+            right = jnp.where((lane_id >= first_one) & (lane_id < first_one + PIECES), moved, 0.0)
+            right = jnp.where(
+                (lane_id >= i * PIECES) & (lane_id < (i + 1) * PIECES), -1.0, right
+            )
+            q_wide[i] = jnp.concatenate([left, right], axis=1).astype(jnp.bfloat16)
+        acc[...] = jnp.zeros_like(acc)
+
+        def step(pair, state, masked):
+            peaks, totals = state
+            keys = jnp.concatenate(
+                [
+                    kv_all[pl.ds(2 * pair, 2), :, :head_width].reshape(span, head_width),
+                    key_gates[pl.ds(2 * pair, 2)].reshape(span, head_width),
+                ],
+                axis=1,
+            )
+            new_peaks, new_totals = [], []
+            for i, (low, high, size) in enumerate(ranges):
+                factor = size**-0.5 * LOG2E
+                scores = lax.dot_general(
+                    keys, q_wide[i], (((1,), (1,)), ((), ())), preferred_element_type=jnp.float32
+                )
+                if masked:
+                    row = lax.broadcasted_iota(jnp.int32, (span, span), 0)
+                    column = lax.broadcasted_iota(jnp.int32, (span, span), 1)
+                    scores = jnp.where(row <= column, scores, -1e30)
+                peak = jnp.maximum(peaks[i], jnp.max(scores, axis=0, keepdims=True))
+                weights = jnp.exp2((scores - peak) * factor)
+                fade = jnp.exp2((peaks[i] - peak) * factor)
+                new_peaks.append(peak)
+                new_totals.append(totals[i] * fade + jnp.sum(weights, axis=0, keepdims=True))
+                acc[low:high, :] = acc[low:high, :] * fade + jnp.dot(
+                    v_turned[pair, low:high, :],
+                    weights.astype(jnp.bfloat16),
+                    preferred_element_type=jnp.float32,
+                )
+            return tuple(new_peaks), tuple(new_totals)
+
+        state = (
+            tuple(jnp.full((1, span), -1e30, jnp.float32) for _ in ranges),
+            tuple(jnp.zeros((1, span), jnp.float32) for _ in ranges),
+        )
+        state = lax.fori_loop(
+            0, double_block, lambda pair, state: step(pair, state, False), state
+        )
+        _, totals = step(double_block, state, True)
+        scaled = jnp.concatenate(
+            [acc[low:high, :] / totals[i] for i, (low, high, _) in enumerate(ranges)], axis=0
+        )
+        attended[pl.ds(2 * tile, 2)] = (
+            scaled.T.astype(jnp.bfloat16).reshape(2, tokens, head_width)
+        )
+        return carry
+
+    lax.fori_loop(0, 2, attend, 0)
+
+    def back_copy(slot, core, place, sp):
+        return remote(
+            attended.at[slot, core * rows : (core + 1) * rows, :],
+            attended_in.at[place],
+            back_sems.at[0, slot, core],
+            back_sems.at[1, 0, place],
+            sp,
+            core,
+        )
+
+    my_place = tp * head_groups + plane
+    for slot in range(4):
+        owner = 2 * tile_double(slot // 2) + slot % 2
+        for core in range(2):
+            here = (owner == me) & (tp == core)
+
+            @pl.when(jnp.logical_not(here))
+            def _():
+                back_copy(slot, core, my_place, owner).start()
+
+            @pl.when(here)
+            def _():
+                attended_in[my_place] = attended[slot, core * rows : (core + 1) * rows, :]
+
+    for h in range(head_groups):
+        own, away = project_copies(h)
+        for copy in own:
+            copy.wait()
+        for copy in away:
+            copy.wait()
+    for h in range(head_groups):
+        for core in range(2):
+            place = core * head_groups + h
+            sender = h * parts + reader_part
+
+            @pl.when(jnp.logical_not((sender == me) & (tp == core)))
+            def _():
+                remote(
+                    attended.at[0, :rows, :],
+                    attended_in.at[place],
+                    back_sems.at[0, 0, 0],
+                    back_sems.at[1, 0, place],
+                    sender,
+                    core,
+                ).wait_recv()
+
+    step_width = return_out.shape[3]
+    chunks = width // step_width
+    joined = jnp.concatenate([attended_in[i] for i in range(2 * head_groups)], axis=1)
+
+    def project_step(n, squares):
+        columns = pl.ds(pl.multiple_of(n * step_width, step_width), step_width)
+        total = residual_ref[:, columns].astype(jnp.float32) + jnp.dot(
+            joined,
+            project[:, :, columns].reshape(2 * head_groups * head_width, step_width),
+            preferred_element_type=jnp.float32,
+        )
+        total = total.astype(jnp.bfloat16).astype(jnp.float32)
+        mixed[:, columns] = total
+        return squares + jnp.sum(total * total, axis=1, keepdims=True)
+
+    squares = lax.fori_loop(0, chunks, project_step, jnp.zeros((rows, 1), jnp.float32))
+    scale = lax.rsqrt(squares / width + 1e-06)
+    scaled_rows = (mixed[...] * scale * gain_ref[...]).astype(jnp.bfloat16)
+    normed[...] = scaled_rows
+    features[tp, local] = scaled_rows
+
+    def across(k, owner):
+        return remote(
+            normed,
+            features.at[tp, owner],
+            across_sems.at[0, k],
+            across_sems.at[1, k],
+            base + (local + k) % group,
+            tp,
+        )
+
+    def beside(k, source, core, owner):
+        return remote(
+            source,
+            features.at[core, owner],
+            beside_sems.at[0, k],
+            beside_sems.at[1, k],
+            me,
+            other,
+        )
+
+    for k in range(1, group):
+        across(k, local).start()
+    beside(0, normed, tp, local).start()
+
+    def pass_on(k, carry):
+        owner = (local + group - k) % group
+        across(k, owner).wait_recv()
+        beside(k, features.at[tp, owner], tp, owner).start()
+        return carry
+
+    lax.fori_loop(1, group, pass_on, 0)
+
+    def receive_pass(k, carry):
+        owner = (local + group - k) % group
+        beside(k, normed, other, owner).wait_recv()
+        return carry
+
+    lax.fori_loop(0, group, receive_pass, 0)
+
+    def wait_weights(which, k):
+        copy = weight_copy(which, k, (me + count - k) % count)
+        copy.wait_recv()
+
+    own_weights[0].wait()
+
+    def wait_up(k, carry):
+        wait_weights(0, k)
+        return carry
+
+    lax.fori_loop(1, count, wait_up, 0)
+    row_groups = 2
+    some = group // row_groups
+
+    def up_step(i, carry):
+        core = (other + i // row_groups) % 2
+        chips = pl.ds((i % row_groups) * some, some)
+        total = jnp.dot(
+            features[core, chips].reshape(some * rows, width),
+            up_all[...].reshape(width, units),
+            preferred_element_type=jnp.float32,
+        )
+        total = jnp.maximum(total, 0.0)
+        hidden[core, chips] = (
+            (total * total).astype(jnp.bfloat16).reshape(some, rows, units)
+        )
+        return carry
+
+    lax.fori_loop(0, 2 * row_groups, up_step, 0)
+    own_weights[1].wait()
+
+    def wait_down(k, carry):
+        wait_weights(1, k)
+        return carry
+
+    lax.fori_loop(1, count, wait_down, 0)
+    per_chunk = count // chunks
+
+    def down_columns(chunk):
+        return jnp.concatenate(
+            [down_all[chunk * per_chunk + i] for i in range(per_chunk)], axis=1
+        )
+
+    def part_copy(chunk):
+        return remote(
+            part_out.at[chunk],
+            part_in.at[chunk],
+            part_sems.at[0, chunk],
+            part_sems.at[1, chunk],
+            me,
+            other,
+        )
+
+    def down_dot(core, chips, chunk):
+        return jnp.dot(
+            hidden[core, chips].reshape(some * rows, units),
+            down_columns(chunk),
+            preferred_element_type=jnp.float32,
+        ).reshape(some, rows, step_width)
+
+    def away_step(chunk, carry):
+        def inner(i, carry):
+            chips = pl.ds(i * some, some)
+            part_out[chunk, chips] = down_dot(other, chips, chunk).astype(jnp.bfloat16)
+            return carry
+
+        lax.fori_loop(0, row_groups, inner, 0)
+        part_copy(chunk).start()
+        return carry
+
+    lax.fori_loop(0, chunks, away_step, 0)
+
+    def return_copy(chunk, k, owner):
+        peer = (local + k) % group
+        return remote(
+            return_out.at[chunk, peer],
+            return_in.at[chunk, owner],
+            return_sems.at[0, chunk, k],
+            return_sems.at[1, chunk, k],
+            base + peer,
+            tp,
+        )
+
+    def home_step(chunk, carry):
+        part_copy(chunk).wait_recv()
+
+        def inner(i, carry):
+            chips = pl.ds(i * some, some)
+            return_out[chunk, chips] = (
+                down_dot(tp, chips, chunk) + part_in[chunk, chips].astype(jnp.float32)
+            ).astype(jnp.bfloat16)
+            return carry
+
+        lax.fori_loop(0, row_groups, inner, 0)
+        for k in range(1, group):
+            return_copy(chunk, k, local).start()
+        return carry
+
+    lax.fori_loop(0, chunks, home_step, 0)
+
+    def final_step(chunk, carry):
+        columns = pl.ds(pl.multiple_of(chunk * step_width, step_width), step_width)
+        total = mixed[:, columns] + return_out[chunk, local].astype(jnp.float32)
+        for k in range(1, group):
+            owner = (local + group - k) % group
+            return_copy(chunk, k, owner).wait_recv()
+            total = total + return_in[chunk, owner].astype(jnp.float32)
+        out_ref[:, columns] = total.astype(jnp.bfloat16)
+        return carry
+
+    lax.fori_loop(0, chunks, final_step, 0)
+
+    for j in range(1, planes):
+        for copy in line_copies(j, me):
+            copy.wait_send()
+    for j in range(planes):
+        for k in range(1, parts):
+            for copy in plane_copies(j, k, kv_send.at[plane], gate_send.at[plane], me):
+                copy.wait_send()
+    for h in range(head_groups):
+        reader = h * parts + reader_part
+
+        @pl.when(reader != me)
+        def _():
+            remote(
+                q_send.at[h], q_all.at[my_slot], q_sems.at[0, h], q_sems.at[1, my_slot], reader, tp
+            ).wait_send()
+
+    for slot in range(4):
+        owner = 2 * tile_double(slot // 2) + slot % 2
+        for core in range(2):
+            here = (owner == me) & (tp == core)
+
+            @pl.when(jnp.logical_not(here))
+            def _():
+                back_copy(slot, core, my_place, owner).wait_send()
+
+    def weights_sent(k, carry):
+        for which in range(2):
+            weight_copy(which, k, me).wait_send()
+        return carry
+
+    lax.fori_loop(1, count, weights_sent, 0)
+    for k in range(1, group):
+        across(k, local).wait_send()
+    for k in range(group):
+        beside(k, normed, tp, local).wait_send()
+
+    def returns_sent(chunk, carry):
+        part_copy(chunk).wait_send()
+        for k in range(1, group):
+            return_copy(chunk, k, local).wait_send()
+        return carry
+
+    lax.fori_loop(0, chunks, returns_sent, 0)
+
+
+def fused_local(
+    residual,
+    queries_narrow,
+    keys_narrow,
+    values_narrow,
+    queries_broad,
+    keys_broad,
+    values_broad,
+    gates_narrow,
+    gates_broad,
+    project_narrow,
+    project_broad,
+    norm_gain,
+    up_weight,
+    down_weight,
+):
+    count = lax.axis_size("sp")
+    group = group_size(count)
+    tokens = queries_narrow.shape[0]
+    rows, width = residual.shape
+    head_groups = gates_broad.shape[1]
+    parts = count // head_groups
+    narrow_heads = gates_narrow.shape[1] // head_groups
+    ranges = head_columns(narrow_heads)
+    heads = len(ranges)
+    head_width = ranges[-1][1]
+    up_rows, unit_total = up_weight.shape
+    units = unit_total // group
+    columns = down_weight.shape[1]
+    step_width = 4 * columns
+    chunks = width // step_width
+    span = 2 * tokens
+    kind = residual.dtype
+    vmem = pl.BlockSpec(memory_space=pltpu.VMEM)
+    anywhere = pl.BlockSpec(memory_space=pl.ANY)
+    dma = pltpu.SemaphoreType.DMA
+    returned = (chunks, group, rows, step_width)
+    return pl.pallas_call(
+        functools.partial(fused_kernel, count, group, head_groups, ranges),
+        out_shape=jax.ShapeDtypeStruct(residual.shape, kind),
+        in_specs=[vmem] * 10 + [anywhere] * 4,
+        out_specs=vmem,
+        scratch_shapes=[
+            pltpu.VMEM((head_groups, tokens, head_width), kind),
+            pltpu.VMEM((head_groups, tokens, 2 * head_width), kind),
+            pltpu.VMEM((head_groups, GATE_ROWS, tokens), kind),
+            pltpu.VMEM((4, tokens, head_width), kind),
+            pltpu.VMEM((count, tokens, 2 * head_width), kind),
+            pltpu.VMEM((count, GATE_ROWS, tokens), kind),
+            pltpu.VMEM((count, tokens, head_width), kind),
+            pltpu.VMEM((count // 2, head_width, span), kind),
+            pltpu.VMEM((heads, span, 2 * head_width), kind),
+            pltpu.VMEM((head_width, span), jnp.float32),
+            pltpu.VMEM((4, tokens, head_width), kind),
+            pltpu.VMEM((2 * head_groups, rows, head_width), kind),
+            pltpu.VMEM((2 * head_groups, head_width, width), kind),
+            pltpu.VMEM((rows, width), jnp.float32),
+            pltpu.VMEM((rows, width), kind),
+            pltpu.VMEM((count, up_rows, units), kind),
+            pltpu.VMEM((count, units, columns), kind),
+            pltpu.VMEM((2, group, rows, width), kind),
+            pltpu.VMEM((2, group, rows, units), kind),
+            pltpu.VMEM(returned, kind),
+            pltpu.VMEM(returned, kind),
+            pltpu.VMEM(returned, kind),
+            pltpu.VMEM(returned, kind),
+            dma((2, head_groups)),
+            dma((2, head_groups)),
+            dma((2, head_groups, parts)),
+            dma((2, head_groups, parts)),
+            dma((2, 4)),
+            dma((2, 4, 2 * head_groups)),
+            dma((head_groups, 2)),
+            dma((2, head_groups, 2)),
+            dma((2, 2, count)),
+            dma((2,)),
+            dma((2, group)),
+            dma((2, group)),
+            dma((2, chunks)),
+            dma((2, chunks, group)),
+        ],
+        compiler_params=pltpu.CompilerParams(
+            collective_id=3, has_side_effects=True, vmem_limit_bytes=60 * 2**20
+        ),
+    )(
+        residual,
+        queries_narrow,
+        keys_narrow,
+        values_narrow,
+        queries_broad,
+        keys_broad,
+        values_broad,
+        gates_narrow,
+        gates_broad,
+        norm_gain.reshape(1, -1),
+        project_narrow,
+        project_broad,
+        up_weight,
+        down_weight,
+    )
+
+
+def layer(*arrays):
+    queries, gates_broad, down_weight = arrays[1], arrays[8], arrays[13]
+    head_groups = gates_broad.shape[1]
+    narrow_heads = arrays[7].shape[1] // head_groups
+    fused = (
+        lax.axis_size("tp") == 2
+        and head_groups == 4
+        and lax.axis_size("sp") == head_groups * 4
+        and narrow_heads * A_DIM + B_DIM == 128
+        and down_weight.shape[1] % 128 == 0
+        and queries.shape[0] % 64 == 0
+    )
+    return fused_local(*arrays) if fused else local(*arrays)
+
+
 def solution(mesh):
     return jax.shard_map(
-        local,
+        layer,
         mesh=mesh,
         in_specs=(
             P(("sp", "tp"), None),

time: 328 us -> 228 us (0.70)
  waiting for transfers between devices: 57.8 us -> 0 us
  between operations: 13.6 us -> 0.01 us
  matrix products: 12.8 us -> 0 us
  other arithmetic: 8.42 us -> 0 us
  local copies, waits for them, and re-layouts: 10.5 us -> 4.01 us
    reduce_scatter x2 -> x0, waiting for transfers between devices: 57.8 us -> none  [the longest x1 38 us: local(): lax.psum_scatter((jnp.dot(attended_narrow, project_narrow, preferred_elem...]
    dot_general x3 -> x0, matrix products: 12.8 us -> none  [the longest x1 11.1 us: local(): down_term = jnp.dot(hidden, down_full, preferred_element_type=jnp.float32)]
    reduce_sum x2 -> x0, other arithmetic: 3.81 us -> none  [the longest x1 2.59 us: local(): summed_rows = jnp.sum(return_parts(parts).astype(jnp.float32), axis=0)]
    pallas_call x3 -> x1, Pallas kernels: 225 us -> 223 us  [fused_local(): pl.pallas_call(functools.partial(fused_kernel, count, group, head_groups,...]
  transfers between devices with their start and end apart: 2 -> 0, of which waited for: 2 -> 0; matrix products, arithmetic and copies ran while one was open for 0% -> 0% of each run, Pallas kernels for 0% -> 0%
where the time goes in v1:
time: 228 us; the launch traced here: 227 us
  Pallas kernels  223 us (98%)
  local copies, waits for them, and re-layouts  4.01 us (2%)
    pallas_call x1, Pallas kernels, fused_local(): pl.pallas_call(functools.partial(fused_kernel, count, group, head_groups,...  223 us

profile of v1, /device:TPU:0, one launch (start us, length us, event | category | flops | bytes accessed | tf_op | source)
XLA Modules:
  0.0 226.6 jit_solution(8974174131852047373)
XLA Ops:
  0.0 0.0 copy-start
  0.0 1.5 copy.15.gn_ref
  1.5 0.0 copy-done
  1.5 0.8 copy.16.gb_ref
  2.2 222.6 %shard_map.136 = bf16[96,2048]{1,0:T(8,128)(2,1)} custom-call(bf16[96,2048]{1,0:T(8,128)(2,1)} %residual_ref.1, bf16[192,256]{1,0:T(8,128)(2,1)} %qn_ref.1, bf16[192,256]{1,0:T(8,128)(2,1)} %kn_ref.1, bf16[192,256]{1,0:T(8,128)(2,1)} %vn_ref.1, bf16[192,256]{1,0:T(8,128)(2,1)} %qb_ref.1, bf16[192,256]{1,0:T(8,128)(2,1)} %kb_ref.1, bf16[192,256]{1,0:T(8,128)(2,1)} %vb_ref.1, ...), custom_call_target="tpu_custom_call" | custom-call | tf_op jit(solution)/shard_map/pallas_call | solution.py:1261
  224.8 1.8 copy.18
Async XLA Ops:
  0.0 1.5 copy-start

commit v2 on v1

--- a/solution.py
+++ b/solution.py
@@ -566,6 +566,7 @@
     return (mixed.astype(jnp.float32) + summed_rows).astype(jnp.bfloat16)
 
 
+IN_FLIGHT = 3
 LOG2E = 1.4426950408889634
 PIECES = 3
 GATE_ROWS = 16
@@ -644,7 +645,8 @@
     back_sems,
     project_own,
     project_sems,
-    weight_sems,
+    share_sems,
+    twin_sems,
     own_sems,
     across_sems,
     beside_sems,
@@ -698,8 +700,7 @@
         ]
 
     narrow_heads = heads - 1
-    gates = pad_lanes(jnp.concatenate([gn_ref[...], gb_ref[...]], axis=1), 128)
-    gates = pad_rows(gates, -(-tokens // 128) * 128).T[:, :tokens]
+    gates = jnp.concatenate([gn_ref[...], gb_ref[...]], axis=0)
     for h in range(head_groups):
         kv_send[h] = jnp.concatenate(
             by_group(kn_ref, kb_ref, h) + by_group(vn_ref, vb_ref, h), axis=1
@@ -830,14 +831,67 @@
     def down_source(chunk):
         return down_ref.at[pl.ds(pl.multiple_of(chunk * units, units), units), :]
 
-    def weight_copy(which, k, owner):
-        peer = (me + k) % count
-        chunk = peer % group
-        source = up_source(chunk) if which == 0 else down_source(chunk)
+    def flip(place, bit):
+        return place + bit * (1 - 2 * ((place // bit) % 2))
+
+    def mate(place, offset):
+        bit = 1
+        while bit <= offset:
+            if offset & bit:
+                place = flip(place, bit)
+            bit *= 2
+        return place
+
+    def share_copy(which, offset, owner):
+        peer = mate(local, offset)
+        source = up_source(peer) if which == 0 else down_source(peer)
         target = up_all.at[owner] if which == 0 else down_all.at[owner]
         return remote(
-            source, target, weight_sems.at[0, which, k], weight_sems.at[1, which, k], peer, tp
-        )
+            source,
+            target,
+            share_sems.at[0, which, offset],
+            share_sems.at[1, which, offset],
+            base + peer,
+            tp,
+        )
+
+    twin = (me + group) % count
+    twin_base = (base + group) % count
+
+    def twin_copy(which, offset):
+        owner = base + mate(local, offset)
+        weights = up_all if which == 0 else down_all
+        if offset:
+            source = weights.at[owner]
+        else:
+            source = up_source(local) if which == 0 else down_source(local)
+        return remote(
+            source,
+            weights.at[owner],
+            twin_sems.at[0, which, offset],
+            twin_sems.at[1, which, offset],
+            twin,
+            tp,
+        )
+
+    far = group // 2
+    near = [offset for offset in range(1, group) if offset != far]
+    near.sort(key=lambda offset: (bin(offset).count("1"), offset))
+    pieces = [(0, 0), (1, 0), (0, far), (1, far)]
+    pieces += [(which, offset) for which in range(2) for offset in near]
+    issued = []
+
+    def tick(amount=1):
+        for _ in range(amount):
+            if len(issued) == len(pieces):
+                return
+            which, offset = pieces[len(issued)]
+            if len(issued) >= IN_FLIGHT:
+                twin_copy(*pieces[len(issued) - IN_FLIGHT]).wait_send()
+            if offset:
+                share_copy(which, offset, base + mate(local, offset)).wait_recv()
+            twin_copy(which, offset).start()
+            issued.append((which, offset))
 
     own_weights = [
         pltpu.make_async_copy(up_source(local), up_all.at[me], own_sems.at[0]),
@@ -845,6 +899,9 @@
     ]
     for copy in own_weights:
         copy.start()
+    for which in range(2):
+        share_copy(which, far, me).start()
+    tick(2)
 
     for j in range(1, planes):
         owner = line_owner(j)
@@ -854,15 +911,10 @@
             for copy in plane_copies(j, k, kv_all.at[owner], gate_all.at[owner], owner):
                 copy.start()
 
-    def start_weights(which):
-        def start(k, carry):
-            weight_copy(which, k, me).start()
-            return carry
-
-        lax.fori_loop(1, count, start, 0)
-
-    start_weights(0)
-    start_weights(1)
+    for which in range(2):
+        for offset in near:
+            share_copy(which, offset, me).start()
+    tick(2)
 
     for j in range(planes):
         for k in range(1, parts):
@@ -956,8 +1008,6 @@
         )
         return carry
 
-    lax.fori_loop(0, 2, attend, 0)
-
     def back_copy(slot, core, place, sp):
         return remote(
             attended.at[slot, core * rows : (core + 1) * rows, :],
@@ -970,6 +1020,10 @@
 
     my_place = tp * head_groups + plane
     for slot in range(4):
+        if slot % 2 == 0:
+            attend(1 - slot // 2, 0)
+            tick()
+        slot = (slot + 2) % 4
         owner = 2 * tile_double(slot // 2) + slot % 2
         for core in range(2):
             here = (owner == me) & (tp == core)
@@ -982,6 +1036,7 @@
             def _():
                 attended_in[my_place] = attended[slot, core * rows : (core + 1) * rows, :]
 
+    tick()
     for h in range(head_groups):
         own, away = project_copies(h)
         for copy in own:
@@ -1025,56 +1080,58 @@
     normed[...] = scaled_rows
     features[tp, local] = scaled_rows
 
-    def across(k, owner):
+    bits = (group // 2, 1 + tp, 2 - tp)
+    levels = len(bits)
+
+    def member(subset):
+        place = local
+        for level in range(levels):
+            if (subset >> level) & 1:
+                place = flip(place, bits[level])
+        return place
+
+    def across(subset):
+        level = subset.bit_length() - 1
+        held = subset - (1 << level)
+        owner = member(held)
         return remote(
-            normed,
+            features.at[tp, owner] if held else normed,
             features.at[tp, owner],
-            across_sems.at[0, k],
-            across_sems.at[1, k],
-            base + (local + k) % group,
+            across_sems.at[0, subset],
+            across_sems.at[1, subset],
+            base + flip(local, bits[level]),
             tp,
         )
 
-    def beside(k, source, core, owner):
+    def beside(subset):
+        owner = member(subset)
         return remote(
-            source,
-            features.at[core, owner],
-            beside_sems.at[0, k],
-            beside_sems.at[1, k],
+            features.at[tp, owner] if subset else normed,
+            features.at[tp, owner],
+            beside_sems.at[0, subset],
+            beside_sems.at[1, subset],
             me,
             other,
         )
 
-    for k in range(1, group):
-        across(k, local).start()
-    beside(0, normed, tp, local).start()
-
-    def pass_on(k, carry):
-        owner = (local + group - k) % group
-        across(k, owner).wait_recv()
-        beside(k, features.at[tp, owner], tp, owner).start()
-        return carry
-
-    lax.fori_loop(1, group, pass_on, 0)
-
-    def receive_pass(k, carry):
-        owner = (local + group - k) % group
-        beside(k, normed, other, owner).wait_recv()
-        return carry
-
-    lax.fori_loop(0, group, receive_pass, 0)
-
-    def wait_weights(which, k):
-        copy = weight_copy(which, k, (me + count - k) % count)
-        copy.wait_recv()
+    def spread(subset):
+        for level in range(subset.bit_length(), levels):
+            across(subset + (1 << level)).start()
+        beside(subset).start()
+
+    spread(0)
+    for subset in range(1, group):
+        across(subset).wait_recv()
+        spread(subset)
+        tick()
+    for subset in range(group):
+        beside(subset).wait_recv()
 
     own_weights[0].wait()
-
-    def wait_up(k, carry):
-        wait_weights(0, k)
-        return carry
-
-    lax.fori_loop(1, count, wait_up, 0)
+    tick(len(pieces))
+    for offset in range(group):
+        twin_copy(0, offset).wait_recv()
+
     row_groups = 2
     some = group // row_groups
 
@@ -1095,11 +1152,9 @@
     lax.fori_loop(0, 2 * row_groups, up_step, 0)
     own_weights[1].wait()
 
-    def wait_down(k, carry):
-        wait_weights(1, k)
-        return carry
-
-    lax.fori_loop(1, count, wait_down, 0)
+    for offset in range(group):
+        twin_copy(1, offset).wait_recv()
+
     per_chunk = count // chunks
 
     def down_columns(chunk):
@@ -1136,14 +1191,14 @@
 
     lax.fori_loop(0, chunks, away_step, 0)
 
-    def return_copy(chunk, k, owner):
-        peer = (local + k) % group
+    def return_copy(chunk, subset):
+        level = subset.bit_length() - 1
         return remote(
-            return_out.at[chunk, peer],
-            return_in.at[chunk, owner],
-            return_sems.at[0, chunk, k],
-            return_sems.at[1, chunk, k],
-            base + peer,
+            return_out.at[chunk, member(subset)],
+            return_in.at[chunk, subset],
+            return_sems.at[0, chunk, subset],
+            return_sems.at[1, chunk, subset],
+            base + flip(local, bits[level]),
             tp,
         )
 
@@ -1158,19 +1213,36 @@
             return carry
 
         lax.fori_loop(0, row_groups, inner, 0)
-        for k in range(1, group):
-            return_copy(chunk, k, local).start()
+        for subset in range(group // 2, group):
+            return_copy(chunk, subset).start()
         return carry
 
     lax.fori_loop(0, chunks, home_step, 0)
+
+    for level in range(levels - 1, 0, -1):
+
+        def merge_step(chunk, carry):
+            for held in range(1 << level):
+                return_copy(chunk, held + (1 << level)).wait_recv()
+                place = member(held)
+                return_out[chunk, place] = (
+                    return_out[chunk, place].astype(jnp.float32)
+                    + return_in[chunk, held + (1 << level)].astype(jnp.float32)
+                ).astype(jnp.bfloat16)
+            for subset in range(1 << (level - 1), 1 << level):
+                return_copy(chunk, subset).start()
+            return carry
+
+        lax.fori_loop(0, chunks, merge_step, 0)
 
     def final_step(chunk, carry):
         columns = pl.ds(pl.multiple_of(chunk * step_width, step_width), step_width)
-        total = mixed[:, columns] + return_out[chunk, local].astype(jnp.float32)
-        for k in range(1, group):
-            owner = (local + group - k) % group
-            return_copy(chunk, k, owner).wait_recv()
-            total = total + return_in[chunk, owner].astype(jnp.float32)
+        return_copy(chunk, 1).wait_recv()
+        total = (
+            mixed[:, columns]
+            + return_out[chunk, local].astype(jnp.float32)
+            + return_in[chunk, 1].astype(jnp.float32)
+        )
         out_ref[:, columns] = total.astype(jnp.bfloat16)
         return carry
 
@@ -1201,21 +1273,20 @@
             def _():
                 back_copy(slot, core, my_place, owner).wait_send()
 
-    def weights_sent(k, carry):
-        for which in range(2):
-            weight_copy(which, k, me).wait_send()
-        return carry
-
-    lax.fori_loop(1, count, weights_sent, 0)
-    for k in range(1, group):
-        across(k, local).wait_send()
-    for k in range(group):
-        beside(k, normed, tp, local).wait_send()
+    for which in range(2):
+        for offset in range(1, group):
+            share_copy(which, offset, me).wait_send()
+    for which, offset in pieces[-IN_FLIGHT:]:
+        twin_copy(which, offset).wait_send()
+    for subset in range(group):
+        if subset:
+            across(subset).wait_send()
+        beside(subset).wait_send()
 
     def returns_sent(chunk, carry):
         part_copy(chunk).wait_send()
-        for k in range(1, group):
-            return_copy(chunk, k, local).wait_send()
+        for subset in range(1, group):
+            return_copy(chunk, subset).wait_send()
         return carry
 
     lax.fori_loop(0, chunks, returns_sent, 0)
@@ -1295,7 +1366,8 @@
             dma((2, 4, 2 * head_groups)),
             dma((head_groups, 2)),
             dma((2, head_groups, 2)),
-            dma((2, 2, count)),
+            dma((2, 2, group)),
+            dma((2, 2, group)),
             dma((2,)),
             dma((2, group)),
             dma((2, group)),
@@ -1313,8 +1385,8 @@
         queries_broad,
         keys_broad,
         values_broad,
-        gates_narrow,
-        gates_broad,
+        gates_narrow.T,
+        gates_broad.T,
         norm_gain.reshape(1, -1),
         project_narrow,
         project_broad,
@@ -1331,6 +1403,7 @@
         lax.axis_size("tp") == 2
         and head_groups == 4
         and lax.axis_size("sp") == head_groups * 4
+        and group_size(lax.axis_size("sp")) == 8
         and narrow_heads * A_DIM + B_DIM == 128
         and down_weight.shape[1] % 128 == 0
         and queries.shape[0] % 64 == 0

time: 228 us -> 175 us (0.77)
  Pallas kernels: 223 us -> 171 us
    pallas_call x1, Pallas kernels: 223 us -> 171 us  [fused_local(): pl.pallas_call(functools.partial(fused_kernel, count, group, head_groups,...]
where the time goes in v2:
time: 175 us; the launch traced here: 173 us
  Pallas kernels  171 us (98%)
  local copies, waits for them, and re-layouts  1.77 us (1%)
    pallas_call x1, Pallas kernels, fused_local(): pl.pallas_call(functools.partial(fused_kernel, count, group, head_groups,...  171 us

profile of v2, /device:TPU:0, one launch (start us, length us, event | category | flops | bytes accessed | tf_op | source)
XLA Modules:
  0.0 172.8 jit_solution(16131740208809513536)
XLA Ops:
  0.0 171.0 %shard_map.136 = bf16[96,2048]{1,0:T(8,128)(2,1)} custom-call(bf16[96,2048]{1,0:T(8,128)(2,1)} %residual_ref.1, bf16[192,256]{1,0:T(8,128)(2,1)} %qn_ref.1, bf16[192,256]{1,0:T(8,128)(2,1)} %kn_ref.1, bf16[192,256]{1,0:T(8,128)(2,1)} %vn_ref.1, bf16[192,256]{1,0:T(8,128)(2,1)} %qb_ref.1, bf16[192,256]{1,0:T(8,128)(2,1)} %kb_ref.1, bf16[192,256]{1,0:T(8,128)(2,1)} %vb_ref.1, ...), custom_call_target="tpu_custom_call" | custom-call | tf_op jit(solution)/shard_map/pallas_call | solution.py:1332
  171.0 1.8 %copy.16 = bf16[96,2048]{1,0:T(8,128)(2,1)} copy(bf16[96,2048]{1,0:T(8,128)(2,1)} %shard_map.136) | data formatting | bytes 786432

commit v3 on v2

--- a/solution.py
+++ b/solution.py
@@ -566,7 +566,7 @@
     return (mixed.astype(jnp.float32) + summed_rows).astype(jnp.bfloat16)
 
 
-IN_FLIGHT = 3
+TICKS = (1, 2, 0, 0, 0, 1, 1, 0, 16, 0)
 LOG2E = 1.4426950408889634
 PIECES = 3
 GATE_ROWS = 16
@@ -618,12 +618,15 @@
     kv_send,
     gate_send,
     q_all,
+    q_gate_all,
     kv_all,
     gate_all,
     key_gates,
     v_turned,
     q_wide,
     acc,
+    peaks,
+    totals,
     attended,
     attended_in,
     project,
@@ -642,6 +645,7 @@
     kv_plane,
     gate_plane,
     q_sems,
+    q_gate_sems,
     back_sems,
     project_own,
     project_sems,
@@ -681,6 +685,17 @@
             device_id_type=pl.DeviceIdType.MESH,
         )
 
+    def flip(place, bit):
+        return place + bit * (1 - 2 * ((place // bit) % 2))
+
+    def mate(place, offset):
+        bit = 1
+        while bit <= offset:
+            if offset & bit:
+                place = flip(place, bit)
+            bit *= 2
+        return place
+
     def hello(k, carry):
         flat = (me * 2 + tp + k) % (count * 2)
         pl.semaphore_signal(
@@ -739,7 +754,7 @@
         return ((plane + planes - j) % planes) * parts + lane
 
     def plane_copies(j, k, kv_source, gate_source, owner):
-        peer = plane * parts + (lane + k) % parts
+        peer = plane * parts + mate(lane, k)
         return (
             remote(
                 kv_source,
@@ -772,6 +787,19 @@
     reader_part = jnp.where(double < parts, double, 2 * parts - 1 - double)
     my_slot = 2 * (double // parts) + me % 2
 
+    def query_copies(h, slot, peer):
+        return (
+            remote(q_send.at[h], q_all.at[slot], q_sems.at[0, h], q_sems.at[1, slot], peer, tp),
+            remote(
+                gate_send.at[h],
+                q_gate_all.at[slot],
+                q_gate_sems.at[0, h],
+                q_gate_sems.at[1, slot],
+                peer,
+                tp,
+            ),
+        )
+
     def tile_double(tile):
         return tile * (2 * parts - 1 - lane) + (1 - tile) * lane
 
@@ -780,13 +808,13 @@
 
         @pl.when(reader != me)
         def _():
-            remote(
-                q_send.at[h], q_all.at[my_slot], q_sems.at[0, h], q_sems.at[1, my_slot], reader, tp
-            ).start()
+            for copy in query_copies(h, my_slot, reader):
+                copy.start()
 
         @pl.when(reader == me)
         def _():
             q_all[my_slot] = q_send[h]
+            q_gate_all[my_slot] = gate_send[h]
 
     def project_pairs(h):
         pairs = []
@@ -831,17 +859,6 @@
     def down_source(chunk):
         return down_ref.at[pl.ds(pl.multiple_of(chunk * units, units), units), :]
 
-    def flip(place, bit):
-        return place + bit * (1 - 2 * ((place // bit) % 2))
-
-    def mate(place, offset):
-        bit = 1
-        while bit <= offset:
-            if offset & bit:
-                place = flip(place, bit)
-            bit *= 2
-        return place
-
     def share_copy(which, offset, owner):
         peer = mate(local, offset)
         source = up_source(peer) if which == 0 else down_source(peer)
@@ -858,7 +875,8 @@
     twin = (me + group) % count
     twin_base = (base + group) % count
 
-    def twin_copy(which, offset):
+    def twin_copy(which, offset, index=None):
+        index = offset if index is None else index
         owner = base + mate(local, offset)
         weights = up_all if which == 0 else down_all
         if offset:
@@ -868,26 +886,24 @@
         return remote(
             source,
             weights.at[owner],
-            twin_sems.at[0, which, offset],
-            twin_sems.at[1, which, offset],
+            twin_sems.at[0, which, index],
+            twin_sems.at[1, which, index],
             twin,
             tp,
         )
 
     far = group // 2
     near = [offset for offset in range(1, group) if offset != far]
-    near.sort(key=lambda offset: (bin(offset).count("1"), offset))
-    pieces = [(0, 0), (1, 0), (0, far), (1, far)]
-    pieces += [(which, offset) for which in range(2) for offset in near]
+    near.sort(key=(1, 6, 5, 2, 3, 7).index)
+    pieces = [(0, 0), (0, far), (1, 0)] + [(0, offset) for offset in near]
+    pieces += [(1, offset) for offset in (1, 2, 3, 4, 6, 5, 7)]
     issued = []
 
-    def tick(amount=1):
+    def tick(amount):
         for _ in range(amount):
             if len(issued) == len(pieces):
                 return
             which, offset = pieces[len(issued)]
-            if len(issued) >= IN_FLIGHT:
-                twin_copy(*pieces[len(issued) - IN_FLIGHT]).wait_send()
             if offset:
                 share_copy(which, offset, base + mate(local, offset)).wait_recv()
             twin_copy(which, offset).start()
@@ -901,7 +917,7 @@
         copy.start()
     for which in range(2):
         share_copy(which, far, me).start()
-    tick(2)
+    tick(TICKS[0])
 
     for j in range(1, planes):
         owner = line_owner(j)
@@ -911,45 +927,31 @@
             for copy in plane_copies(j, k, kv_all.at[owner], gate_all.at[owner], owner):
                 copy.start()
 
-    for which in range(2):
-        for offset in near:
-            share_copy(which, offset, me).start()
-    tick(2)
-
-    for j in range(planes):
-        for k in range(1, parts):
-            owner = ((plane + planes - j) % planes) * parts + (lane + parts - k) % parts
-            for copy in plane_copies(j, k, kv_all.at[owner], gate_all.at[owner], owner):
-                copy.wait_recv()
-
-    def turn(pair, carry):
-        values = kv_all[pl.ds(2 * pair, 2), :, head_width:].reshape(span, head_width)
-        v_turned[pair] = values.astype(jnp.float32).T.astype(jnp.bfloat16)
-        for i in range(2):
-            block = pad_rows(gate_all[2 * pair + i].astype(jnp.float32), 128)
-            block = pad_lanes(block, -(-tokens // 128) * 128).T[:tokens]
-            key_gates[2 * pair + i] = block.astype(jnp.bfloat16)
-        return carry
-
-    lax.fori_loop(0, count // 2, turn, 0)
+    for offset in near:
+        share_copy(0, offset, me).start()
+    for offset in (1, 2, 3, 6, 5, 7):
+        share_copy(1, offset, me).start()
+    tick(TICKS[1])
 
     for slot in range(4):
         owner = 2 * tile_double(slot // 2) + slot % 2
 
         @pl.when(owner != me)
         def _():
-            remote(
-                q_send.at[0], q_all.at[slot], q_sems.at[0, 0], q_sems.at[1, slot], owner, tp
-            ).wait_recv()
+            for copy in query_copies(0, slot, owner):
+                copy.wait_recv()
 
     lane_id = lax.broadcasted_iota(jnp.int32, (span, head_width), 1)
     first_one = heads * PIECES
 
-    def attend(tile, carry):
-        double_block = tile_double(tile)
+    def turned_gates(lines):
+        block = pad_lanes(pad_rows(lines.astype(jnp.float32), 128), -(-tokens // 128) * 128)
+        return block.T[:tokens]
+
+    def widen(tile, carry):
         query = q_all[pl.ds(2 * tile, 2)].reshape(span, head_width).astype(jnp.float32)
-        own_gates = (
-            key_gates[pl.ds(2 * double_block, 2)].reshape(span, head_width).astype(jnp.float32)
+        own_gates = jnp.concatenate(
+            [turned_gates(q_gate_all[2 * tile + i]) for i in range(2)], axis=0
         )
         for i, (low, high, _) in enumerate(ranges):
             left = jnp.where((lane_id >= low) & (lane_id < high), query, 0.0)
@@ -958,55 +960,89 @@
             right = jnp.where(
                 (lane_id >= i * PIECES) & (lane_id < (i + 1) * PIECES), -1.0, right
             )
-            q_wide[i] = jnp.concatenate([left, right], axis=1).astype(jnp.bfloat16)
-        acc[...] = jnp.zeros_like(acc)
-
-        def step(pair, state, masked):
-            peaks, totals = state
-            keys = jnp.concatenate(
-                [
-                    kv_all[pl.ds(2 * pair, 2), :, :head_width].reshape(span, head_width),
-                    key_gates[pl.ds(2 * pair, 2)].reshape(span, head_width),
-                ],
-                axis=1,
+            q_wide[tile, i] = jnp.concatenate([left, right], axis=1).astype(jnp.bfloat16)
+        acc[tile] = jnp.zeros((head_width, span), jnp.float32)
+        peaks[tile] = jnp.full((heads, 1, span), -1e30, jnp.float32)
+        totals[tile] = jnp.zeros((heads, 1, span), jnp.float32)
+        return carry
+
+    lax.fori_loop(0, 2, widen, 0)
+
+    def turn(pair):
+        values = kv_all[pl.ds(2 * pair, 2), :, head_width:].reshape(span, head_width)
+        v_turned[pair] = values.astype(jnp.float32).T.astype(jnp.bfloat16)
+        for i in range(2):
+            key_gates[2 * pair + i] = turned_gates(gate_all[2 * pair + i]).astype(jnp.bfloat16)
+
+    def attend(tile, pair, masked):
+        keys = jnp.concatenate(
+            [
+                kv_all[pl.ds(2 * pair, 2), :, :head_width].reshape(span, head_width),
+                key_gates[pl.ds(2 * pair, 2)].reshape(span, head_width),
+            ],
+            axis=1,
+        )
+        for i, (low, high, size) in enumerate(ranges):
+            factor = size**-0.5 * LOG2E
+            scores = lax.dot_general(
+                keys, q_wide[tile, i], (((1,), (1,)), ((), ())), preferred_element_type=jnp.float32
             )
-            new_peaks, new_totals = [], []
-            for i, (low, high, size) in enumerate(ranges):
-                factor = size**-0.5 * LOG2E
-                scores = lax.dot_general(
-                    keys, q_wide[i], (((1,), (1,)), ((), ())), preferred_element_type=jnp.float32
-                )
-                if masked:
-                    row = lax.broadcasted_iota(jnp.int32, (span, span), 0)
-                    column = lax.broadcasted_iota(jnp.int32, (span, span), 1)
-                    scores = jnp.where(row <= column, scores, -1e30)
-                peak = jnp.maximum(peaks[i], jnp.max(scores, axis=0, keepdims=True))
-                weights = jnp.exp2((scores - peak) * factor)
-                fade = jnp.exp2((peaks[i] - peak) * factor)
-                new_peaks.append(peak)
-                new_totals.append(totals[i] * fade + jnp.sum(weights, axis=0, keepdims=True))
-                acc[low:high, :] = acc[low:high, :] * fade + jnp.dot(
-                    v_turned[pair, low:high, :],
-                    weights.astype(jnp.bfloat16),
-                    preferred_element_type=jnp.float32,
-                )
-            return tuple(new_peaks), tuple(new_totals)
-
-        state = (
-            tuple(jnp.full((1, span), -1e30, jnp.float32) for _ in ranges),
-            tuple(jnp.zeros((1, span), jnp.float32) for _ in ranges),
-        )
-        state = lax.fori_loop(
-            0, double_block, lambda pair, state: step(pair, state, False), state
-        )
-        _, totals = step(double_block, state, True)
+            if masked:
+                row = lax.broadcasted_iota(jnp.int32, (span, span), 0)
+                column = lax.broadcasted_iota(jnp.int32, (span, span), 1)
+                scores = jnp.where(row <= column, scores, -1e30)
+            before = peaks[tile, i]
+            peak = jnp.maximum(before, jnp.max(scores, axis=0, keepdims=True))
+            weights = jnp.exp2((scores - peak) * factor)
+            fade = jnp.exp2((before - peak) * factor)
+            peaks[tile, i] = peak
+            totals[tile, i] = totals[tile, i] * fade + jnp.sum(weights, axis=0, keepdims=True)
+            acc[tile, low:high, :] = acc[tile, low:high, :] * fade + jnp.dot(
+                v_turned[pair, low:high, :],
+                weights.astype(jnp.bfloat16),
+                preferred_element_type=jnp.float32,
+            )
+
+    for j in range(planes):
+        source_plane = (plane + planes - j) % planes
+        for k in range(1, parts):
+            owner = source_plane * parts + mate(lane, k)
+            for copy in plane_copies(j, k, kv_all.at[owner], gate_all.at[owner], owner):
+                copy.wait_recv()
+
+        def visit(i, carry):
+            pair = source_plane * (parts // 2) + i // 2
+            tile = i % 2
+            double_block = tile_double(tile)
+
+            @pl.when(tile == 0)
+            def _():
+                turn(pair)
+
+            @pl.when(pair < double_block)
+            def _():
+                attend(tile, pair, False)
+
+            @pl.when(pair == double_block)
+            def _():
+                attend(tile, pair, True)
+
+            return carry
+
+        lax.fori_loop(0, parts, visit, 0)
+        tick(TICKS[2 + j])
+
+    def settle(tile, carry):
         scaled = jnp.concatenate(
-            [acc[low:high, :] / totals[i] for i, (low, high, _) in enumerate(ranges)], axis=0
+            [acc[tile, low:high, :] / totals[tile, i] for i, (low, high, _) in enumerate(ranges)],
+            axis=0,
         )
         attended[pl.ds(2 * tile, 2)] = (
             scaled.T.astype(jnp.bfloat16).reshape(2, tokens, head_width)
         )
         return carry
+
+    lax.fori_loop(0, 2, settle, 0)
 
     def back_copy(slot, core, place, sp):
         return remote(
@@ -1020,10 +1056,6 @@
 
     my_place = tp * head_groups + plane
     for slot in range(4):
-        if slot % 2 == 0:
-            attend(1 - slot // 2, 0)
-            tick()
-        slot = (slot + 2) % 4
         owner = 2 * tile_double(slot // 2) + slot % 2
         for core in range(2):
             here = (owner == me) & (tp == core)
@@ -1036,7 +1068,7 @@
             def _():
                 attended_in[my_place] = attended[slot, core * rows : (core + 1) * rows, :]
 
-    tick()
+    tick(TICKS[6])
     for h in range(head_groups):
         own, away = project_copies(h)
         for copy in own:
@@ -1074,6 +1106,7 @@
         mixed[:, columns] = total
         return squares + jnp.sum(total * total, axis=1, keepdims=True)
 
+    tick(TICKS[7])
     squares = lax.fori_loop(0, chunks, project_step, jnp.zeros((rows, 1), jnp.float32))
     scale = lax.rsqrt(squares / width + 1e-06)
     scaled_rows = (mixed[...] * scale * gain_ref[...]).astype(jnp.bfloat16)
@@ -1120,24 +1153,18 @@
         beside(subset).start()
 
     spread(0)
-    for subset in range(1, group):
+    tick(TICKS[8])
+    for subset in (2, 1, 3):
         across(subset).wait_recv()
         spread(subset)
-        tick()
-    for subset in range(group):
-        beside(subset).wait_recv()
-
+        tick(TICKS[9])
+    tick(len(pieces))
     own_weights[0].wait()
-    tick(len(pieces))
-    for offset in range(group):
-        twin_copy(0, offset).wait_recv()
-
     row_groups = 2
     some = group // row_groups
 
-    def up_step(i, carry):
-        core = (other + i // row_groups) % 2
-        chips = pl.ds((i % row_groups) * some, some)
+    def up_step(core, place):
+        chips = pl.ds(place * some, some)
         total = jnp.dot(
             features[core, chips].reshape(some * rows, width),
             up_all[...].reshape(width, units),
@@ -1147,15 +1174,40 @@
         hidden[core, chips] = (
             (total * total).astype(jnp.bfloat16).reshape(some, rows, units)
         )
-        return carry
-
-    lax.fori_loop(0, 2 * row_groups, up_step, 0)
+
+    home = local // some
+    for subset in (4, 6):
+        across(subset).wait_recv()
+        spread(subset)
+    for subset in (0, 2, 4, 6):
+        beside(subset).wait_recv()
+    for offset in range(group):
+        twin_copy(0, offset).wait_recv()
+
+    def up_both(place):
+        def inner(core, carry):
+            up_step(core, place)
+            return carry
+
+        lax.fori_loop(0, 2, inner, 0)
+
+    up_both(home)
+    for subset in (5, 7):
+        across(subset).wait_recv()
+        spread(subset)
+    for subset in (1, 3, 5, 7):
+        beside(subset).wait_recv()
+    up_both(1 - home)
     own_weights[1].wait()
-
-    for offset in range(group):
-        twin_copy(1, offset).wait_recv()
-
     per_chunk = count // chunks
+
+    def chunk_of(i):
+        return ((base + (i // 2) * group) % count) // per_chunk + (local // per_chunk + i) % 2
+
+    def wait_down(i):
+        if i >= chunks // 2:
+            for k in range(per_chunk):
+                twin_copy(1, (i % 2) * per_chunk + k).wait_recv()
 
     def down_columns(chunk):
         return jnp.concatenate(
@@ -1179,7 +1231,7 @@
             preferred_element_type=jnp.float32,
         ).reshape(some, rows, step_width)
 
-    def away_step(chunk, carry):
+    def away_step(chunk):
         def inner(i, carry):
             chips = pl.ds(i * some, some)
             part_out[chunk, chips] = down_dot(other, chips, chunk).astype(jnp.bfloat16)
@@ -1187,9 +1239,7 @@
 
         lax.fori_loop(0, row_groups, inner, 0)
         part_copy(chunk).start()
-        return carry
-
-    lax.fori_loop(0, chunks, away_step, 0)
+
 
     def return_copy(chunk, subset):
         level = subset.bit_length() - 1
@@ -1202,7 +1252,7 @@
             tp,
         )
 
-    def home_step(chunk, carry):
+    def home_step(chunk):
         part_copy(chunk).wait_recv()
 
         def inner(i, carry):
@@ -1215,13 +1265,19 @@
         lax.fori_loop(0, row_groups, inner, 0)
         for subset in range(group // 2, group):
             return_copy(chunk, subset).start()
-        return carry
-
-    lax.fori_loop(0, chunks, home_step, 0)
+
+    wait_down(0)
+    away_step(chunk_of(0))
+    for i in range(chunks):
+        if i + 1 < chunks:
+            wait_down(i + 1)
+            away_step(chunk_of(i + 1))
+        home_step(chunk_of(i))
 
     for level in range(levels - 1, 0, -1):
 
-        def merge_step(chunk, carry):
+        def merge_step(i, carry):
+            chunk = chunk_of(i)
             for held in range(1 << level):
                 return_copy(chunk, held + (1 << level)).wait_recv()
                 place = member(held)
@@ -1235,7 +1291,8 @@
 
         lax.fori_loop(0, chunks, merge_step, 0)
 
-    def final_step(chunk, carry):
+    def final_step(i, carry):
+        chunk = chunk_of(i)
         columns = pl.ds(pl.multiple_of(chunk * step_width, step_width), step_width)
         return_copy(chunk, 1).wait_recv()
         total = (
@@ -1260,9 +1317,8 @@
 
         @pl.when(reader != me)
         def _():
-            remote(
-                q_send.at[h], q_all.at[my_slot], q_sems.at[0, h], q_sems.at[1, my_slot], reader, tp
-            ).wait_send()
+            for copy in query_copies(h, my_slot, reader):
+                copy.wait_send()
 
     for slot in range(4):
         owner = 2 * tile_double(slot // 2) + slot % 2
@@ -1276,7 +1332,7 @@
     for which in range(2):
         for offset in range(1, group):
             share_copy(which, offset, me).wait_send()
-    for which, offset in pieces[-IN_FLIGHT:]:
+    for which, offset in pieces:
         twin_copy(which, offset).wait_send()
     for subset in range(group):
         if subset:
@@ -1339,12 +1395,15 @@
             pltpu.VMEM((head_groups, tokens, 2 * head_width), kind),
             pltpu.VMEM((head_groups, GATE_ROWS, tokens), kind),
             pltpu.VMEM((4, tokens, head_width), kind),
+            pltpu.VMEM((4, GATE_ROWS, tokens), kind),
             pltpu.VMEM((count, tokens, 2 * head_width), kind),
             pltpu.VMEM((count, GATE_ROWS, tokens), kind),
             pltpu.VMEM((count, tokens, head_width), kind),
             pltpu.VMEM((count // 2, head_width, span), kind),
-            pltpu.VMEM((heads, span, 2 * head_width), kind),
-            pltpu.VMEM((head_width, span), jnp.float32),
+            pltpu.VMEM((2, heads, span, 2 * head_width), kind),
+            pltpu.VMEM((2, head_width, span), jnp.float32),
+            pltpu.VMEM((2, heads, 1, span), jnp.float32),
+            pltpu.VMEM((2, heads, 1, span), jnp.float32),
             pltpu.VMEM((4, tokens, head_width), kind),
             pltpu.VMEM((2 * head_groups, rows, head_width), kind),
             pltpu.VMEM((2 * head_groups, head_width, width), kind),
@@ -1362,6 +1421,7 @@
             dma((2, head_groups)),
             dma((2, head_groups, parts)),
             dma((2, head_groups, parts)),
+            dma((2, 4)),
             dma((2, 4)),
             dma((2, 4, 2 * head_groups)),
             dma((head_groups, 2)),

time: 175 us -> 160 us (0.914); the launches traced: 173 us -> 160 us
  Pallas kernels: 171 us -> 158 us
    pallas_call x1, Pallas kernels: 171 us -> 158 us  [fused_local(): pl.pallas_call(functools.partial(fused_kernel, count, group, head_groups,...]
where the time goes in v3:
time: 160 us
  Pallas kernels  158 us (99%)
  local copies, waits for them, and re-layouts  1.77 us (1%)
    pallas_call x1, Pallas kernels, fused_local(): pl.pallas_call(functools.partial(fused_kernel, count, group, head_groups,...  158 us

profile of v3, /device:TPU:0, one launch (start us, length us, event | category | flops | bytes accessed | tf_op | source)
XLA Modules:
  0.0 159.7 jit_solution(4496705075378360703)
XLA Ops:
  0.0 157.9 %shard_map.136 = bf16[96,2048]{1,0:T(8,128)(2,1)} custom-call(bf16[96,2048]{1,0:T(8,128)(2,1)} %residual_ref.1, bf16[192,256]{1,0:T(8,128)(2,1)} %qn_ref.1, bf16[192,256]{1,0:T(8,128)(2,1)} %kn_ref.1, bf16[192,256]{1,0:T(8,128)(2,1)} %vn_ref.1, bf16[192,256]{1,0:T(8,128)(2,1)} %qb_ref.1, bf16[192,256]{1,0:T(8,128)(2,1)} %kb_ref.1, bf16[192,256]{1,0:T(8,128)(2,1)} %vb_ref.1, ...), custom_call_target="tpu_custom_call" | custom-call | tf_op jit(solution)/shard_map/pallas_call | solution.py:1388
  157.9 1.8 %copy.16 = bf16[96,2048]{1,0:T(8,128)(2,1)} copy(bf16[96,2048]{1,0:T(8,128)(2,1)} %shard_map.136) | data formatting | bytes 786432

commit v4 on v3

--- a/solution.py
+++ b/solution.py
@@ -566,7 +566,7 @@
     return (mixed.astype(jnp.float32) + summed_rows).astype(jnp.bfloat16)
 
 
-TICKS = (1, 2, 0, 0, 0, 1, 1, 0, 16, 0)
+TICKS = (1, 3, 0, 0, 0, 1, 2, 0, 16, 0)
 LOG2E = 1.4426950408889634
 PIECES = 3
 GATE_ROWS = 16
@@ -895,8 +895,8 @@
     far = group // 2
     near = [offset for offset in range(1, group) if offset != far]
     near.sort(key=(1, 6, 5, 2, 3, 7).index)
-    pieces = [(0, 0), (0, far), (1, 0)] + [(0, offset) for offset in near]
-    pieces += [(1, offset) for offset in (1, 2, 3, 4, 6, 5, 7)]
+    pieces = [(0, 0), (0, far), (1, 0), (1, far)] + [(0, offset) for offset in near]
+    pieces += [(1, offset) for offset in (1, 2, 3, 6, 5, 7)]
     issued = []
 
     def tick(amount):
@@ -929,8 +929,6 @@
 
     for offset in near:
         share_copy(0, offset, me).start()
-    for offset in (1, 2, 3, 6, 5, 7):
-        share_copy(1, offset, me).start()
     tick(TICKS[1])
 
     for slot in range(4):
@@ -1068,6 +1066,8 @@
             def _():
                 attended_in[my_place] = attended[slot, core * rows : (core + 1) * rows, :]
 
+    for offset in (1, 2, 3, 6, 5, 7):
+        share_copy(1, offset, me).start()
     tick(TICKS[6])
     for h in range(head_groups):
         own, away = project_copies(h)

time: 160 us -> 151 us (0.944)
  Pallas kernels: 158 us -> 149 us
    pallas_call x1, Pallas kernels: 158 us -> 149 us  [fused_local(): pl.pallas_call(functools.partial(fused_kernel, count, group, head_groups,...]
where the time goes in v4:
time: 151 us
  Pallas kernels  149 us (99%)
  local copies, waits for them, and re-layouts  1.77 us (1%)
    pallas_call x1, Pallas kernels, fused_local(): pl.pallas_call(functools.partial(fused_kernel, count, group, head_groups,...  149 us

profile of v4, /device:TPU:0, one launch (start us, length us, event | category | flops | bytes accessed | tf_op | source)
XLA Modules:
  0.0 150.6 jit_solution(3664171011180612705)
XLA Ops:
  0.0 148.8 %shard_map.136 = bf16[96,2048]{1,0:T(8,128)(2,1)} custom-call(bf16[96,2048]{1,0:T(8,128)(2,1)} %residual_ref.1, bf16[192,256]{1,0:T(8,128)(2,1)} %qn_ref.1, bf16[192,256]{1,0:T(8,128)(2,1)} %kn_ref.1, bf16[192,256]{1,0:T(8,128)(2,1)} %vn_ref.1, bf16[192,256]{1,0:T(8,128)(2,1)} %qb_ref.1, bf16[192,256]{1,0:T(8,128)(2,1)} %kb_ref.1, bf16[192,256]{1,0:T(8,128)(2,1)} %vb_ref.1, ...), custom_call_target="tpu_custom_call" | custom-call | tf_op jit(solution)/shard_map/pallas_call | solution.py:1388
  148.8 1.8 %copy.16 = bf16[96,2048]{1,0:T(8,128)(2,1)} copy(bf16[96,2048]{1,0:T(8,128)(2,1)} %shard_map.136) | data formatting | bytes 786432
